TPU v7x, 32 devices: a whole 2x2x4 slice. The times are simulated.
32 devices in a mesh: sp: 16 (over z, y, x), tp: 2 (over core).
Axes of the slice: x: 2, y: 2, z: 4, core: 2. Of those that a mesh axis runs over, the one named last changes fastest.
Arguments:
- value_in: bfloat16 [4096, 2048], P('sp', 'tp'), may hold values from -25 to 25, as said below
- gate_in: bfloat16 [4096, 2048], P('sp', 'tp'), may hold values from -6 to 6
- taps: float32 [31, 2048], P(None, 'tp'), may hold values from -1 to 1
- gain: float32 [2048], P('tp'), may hold values from 0.1 to 1.9
- shift: float32 [2048], P('tp'), may hold values from -3 to 3
- w_out: bfloat16 [2048, 2048], P('tp'), may hold values from -0.125 to 0.125
- grad_out: bfloat16 [4096, 2048], P('sp'), may hold values from -6 to 6
Outputs:
- d_value: bfloat16 [4096, 2048], P('sp', 'tp')
- d_gate: bfloat16 [4096, 2048], P('sp', 'tp')
- d_taps: float32 [31, 2048], P(None, 'tp')
- d_gain: float32 [2048], P('tp')
- d_shift: float32 [2048], P('tp')
Inputs may be any that keep to these rules, and one draw needn't show every extreme that they name: `value_in`: channel blocks of different magnitude.
All inputs are finite; a program needn't handle non-finite values.
Results may differ from a plain program's by a relative error of at most 0.007.
Values may be sent and summed in bfloat16 or wider, within the bound.
No kernel may reach another device: no remote copies, remote signals or barrier semaphores. Data moves between devices by JAX's collectives and lax.ppermute only.
A program may use at most 64 MiB of HBM per device.

v0:
```python
import math
import jax
import jax.numpy as jnp
from jax import lax
from jax.sharding import PartitionSpec as P

EPS = 1e-05


def with_halo(block, sides, width):
    for axis, dim in sides:
        count = lax.axis_size(axis)
        forward = [(i, i + 1) for i in range(count - 1)]
        backward = [(target, source) for source, target in forward]
        low = lax.ppermute(
            lax.slice_in_dim(block, block.shape[dim] - width, None, axis=dim), axis, forward
        )
        high = lax.ppermute(lax.slice_in_dim(block, 0, width, axis=dim), axis, backward)
        block = jnp.concatenate([low, block, high], axis=dim)
    return block


def gated_rows(value_rows, gate_rows):
    gate_sig = jax.nn.sigmoid(gate_rows.astype(jnp.float32))
    return ((value_rows.astype(jnp.float32) * gate_sig).astype(jnp.bfloat16), gate_sig)


def convolve(window, taps, count):
    wide = window.astype(jnp.float32)
    total = jnp.zeros((count, wide.shape[1]), jnp.float32)
    for offset in range(taps.shape[0]):
        total = total + taps[offset] * wide[offset : offset + count]
    return total


def norm_backward(conv_out, grad_rows, gain, shift, w_out, width):
    sums, squares = lax.psum((jnp.sum(conv_out, 1), jnp.sum(conv_out * conv_out, 1)), "tp")
    mean = sums / width
    var = squares / width - mean * mean
    inv = lax.rsqrt(var + EPS)
    normed = (conv_out - mean[:, None]) * inv[:, None]
    pre = normed * gain + shift
    grad_mix = lax.dot_general(
        grad_rows, w_out, (((1,), (1,)), ((), ())), preferred_element_type=jnp.float32
    )
    sig = jax.nn.sigmoid(pre)
    grad_pre = grad_mix * sig * (1.0 + pre * (1.0 - sig))
    grad_normed = grad_pre * gain
    first, second = lax.psum((jnp.sum(grad_normed, 1), jnp.sum(grad_normed * normed, 1)), "tp")
    grad_conv = inv[:, None] * (
        grad_normed - first[:, None] / width - normed * second[:, None] / width
    )
    return (grad_conv, grad_pre, normed)


def shards(value_in, gate_in, taps, gain, shift, w_out, grad_out):
    half = taps.shape[0] // 2
    kernel = taps.shape[0]
    rows = value_in.shape[0]
    width = value_in.shape[1] * lax.axis_size("tp")
    total = rows * lax.axis_size("sp")
    gated, gate_sig = gated_rows(value_in, gate_in)
    gated_wide = with_halo(gated, (("sp", 0),), half)
    conv_out = convolve(gated_wide, taps, rows)
    grad_conv, grad_pre, normed = norm_backward(conv_out, grad_out, gain, shift, w_out, width)
    grad_wide = with_halo(grad_conv, (("sp", 0),), half)
    own_grad = grad_wide[half : half + rows]
    gated_float = gated_wide.astype(jnp.float32)
    grad_gated = jnp.zeros((rows, own_grad.shape[1]), jnp.float32)
    for offset in range(kernel):
        grad_gated = (
            grad_gated + taps[offset] * grad_wide[2 * half - offset : 2 * half - offset + rows]
        )
    tap_terms = jnp.stack(
        [jnp.sum(own_grad * gated_float[offset : offset + rows], 0) for offset in range(kernel)]
    )
    scale = 1.0 / math.sqrt(total)
    stacked = (
        jnp.concatenate(
            [tap_terms, jnp.sum(grad_pre * normed, 0)[None], jnp.sum(grad_pre, 0)[None]], 0
        )
        * scale
    )
    summed = lax.psum(stacked, "sp")
    d_taps = summed[:kernel]
    d_gain = summed[kernel]
    d_shift = summed[kernel + 1]
    d_value = (grad_gated * gate_sig).astype(jnp.bfloat16)
    d_gate = (grad_gated * value_in.astype(jnp.float32) * gate_sig * (1.0 - gate_sig)).astype(
        jnp.bfloat16
    )
    return (d_value, d_gate, d_taps, d_gain, d_shift)


def solution(mesh):
    return jax.shard_map(
        shards,
        mesh=mesh,
        in_specs=(
            P("sp", "tp"),
            P("sp", "tp"),
            P(None, "tp"),
            P("tp"),
            P("tp"),
            P("tp", None),
            P("sp", None),
        ),
        out_specs=(P("sp", "tp"), P("sp", "tp"), P(None, "tp"), P("tp"), P("tp")),
        check_vma=False,
    )
```

profile of v0, /device:TPU:0, one launch (start us, length us, event | category | flops | bytes accessed | tf_op | source)
XLA Modules:
  0.0 175.2 jit_solution(298959568165321427)
XLA Ops:
  7.2 0.0 all-reduce.4.cloned.1.call-start
  7.2 1.6 fusion.1
  8.9 4.9 %collective-permute-start = (bf16[15,1024]{1,0:T(8,128)(2,1)S(1)}, bf16[15,1024]{1,0:T(8,128)(2,1)S(1)}, u32[]{:S(2)}, u32[]{:S(2)}) collective-permute-start(bf16[15,1024]{1,0:T(8,128)(2,1)S(1)} %get-tuple-element.52), channel_id=1, source_target_pairs={{0,2},{2,4},{4,6},{6,8},{8,10},{10,12},{12,14},{14,16},{16,18},{18... | collective-permute-start | bytes 92168 | tf_op jit(solution)/shard_map/ppermute | solution.py:15
  13.7 1.3 collective-permute-start.1
  15.0 0.1 fusion.97
  15.4 4.2 %collective-permute-done.1 = bf16[15,1024]{1,0:T(8,128)(2,1)S(1)} collective-permute-done((bf16[15,1024]{1,0:T(8,128)(2,1)S(1)}, bf16[15,1024]{1,0:T(8,128)(2,1)S(1)}, u32[]{:S(2)}, u32[]{:S(2)}) %collective-permute-start.1) | collective-permute-done | bytes 30752 | tf_op jit(solution)/shard_map/ppermute | solution.py:18
  19.5 0.2 maximum_convert_fusion
  19.7 5.7 %multiply_reduce_fusion.33 = (f32[256]{0:T(256)S(1)}, f32[256]{0:T(256)S(1)}, f32[256,1024]{1,0:T(8,128)S(1)}) fusion(f32[286,1024]{1,0:T(8,128)S(1)} %maximum_convert_fusion, f32[1024]{0:T(1024)S(1)} %bitcast.126, f32[1024]{0:T(1024)S(1)} %bitcast.128, f32[1024]{0:T(1024)S(1)} %bitcast.70, f32[1024]{0:T(1024)S(1)} %bitcast.72, f32[1024]{0:T(1024)S(1)} %bitcast.74, ...), kind=kLoop, calls=%fused_computation.186 | loop fusion | flops 16776704 | bytes 33683456 | tf_op jit(solution)/shard_map/reduce_sum | solution.py:37
  25.6 2.5 %all-reduce.1 = (f32[256]{0:T(256)S(1)}, f32[256]{0:T(256)S(1)}) all-reduce(f32[256]{0:T(256)S(1)} %get-tuple-element.41, f32[256]{0:T(256)S(1)} %get-tuple-element.40), channel_id=1, replica_groups=mesh['sp'=16,'tp'=2] {'tp'}, use_global_device_ids=true, to_apply=%region_3.0 | all-reduce | flops 512 | bytes 4096 | tf_op jit(solution)/shard_map/psum | solution.py:37
  28.1 5.5 %multiply_reduce_fusion = (f32[1024]{0:T(1024)}, f32[256]{0:T(256)S(1)}, f32[256]{0:T(256)S(1)}, f32[1024]{0:T(1024)}, f32[256,1024]{1,0:T(8,128)}) fusion(f32[256,1024]{1,0:T(8,128)S(1)} %get-tuple-element.49, f32[256]{0:T(256)S(1)} %get-tuple-element.88, f32[256]{0:T(256)S(1)} %get-tuple-element.87, f32[1024]{0:T(1024)S(1)} %copy-done.24, ...), kind=kOutput, calls=%fused_computation.150 | convolution fusion | flops 1078720000 | bytes 7360512 | tf_op jit(solution)/shard_map/dot_general | solution.py:43
  33.7 2.4 %all-reduce = (f32[256]{0:T(256)S(1)}, f32[256]{0:T(256)S(1)}) all-reduce(f32[256]{0:T(256)S(1)} %get-tuple-element.37, f32[256]{0:T(256)S(1)} %get-tuple-element.38), channel_id=1, replica_groups=mesh['sp'=16,'tp'=2] {'tp'}, use_global_device_ids=true, to_apply=%region_7.0 | all-reduce | flops 512 | bytes 4096 | tf_op jit(solution)/shard_map/psum | solution.py:49
  36.1 4.8 %multiply_reduce_fusion.1 = (f32[1024]{0:T(1024)}, f32[1024]{0:T(1024)}, f32[1024]{0:T(1024)}, f32[1024]{0:T(1024)}, f32[1024]{0:T(1024)}, /*index=5*/f32[1024]{...) fusion(f32[286,1024]{1,0:T(8,128)S(1)} %maximum_convert_fusion,, ...), kind=kLoop, calls=%fused_computation.151 | loop fusion | flops 11515904 | bytes 22102016 | tf_op jit(solution)/shard_map/reduce_sum | solution.py:75
  41.0 2.4 %multiply_reduce_fusion.2 = (f32[1024]{0:T(1024)}, f32[1024]{0:T(1024)}, f32[1024]{0:T(1024)}, f32[1024]{0:T(1024)}, f32[1024]{0:T(1024)}, /*index=5*/f32[1024]{...) fusion(f32[256,1024]{1,0:T(8,128)S(1)} %get-tuple-element.46, ...), kind=kLoop, calls=%fused_computation.152 | loop fusion | flops 6802432 | bytes 14733312 | tf_op jit(solution)/shard_map/reduce_sum | solution.py:75
  43.3 0.6 fusion.94
  44.0 1.3 collective-permute-start.2
  45.3 4.9 %collective-permute-start.3 = (f32[15,1024]{1,0:T(8,128)S(1)}, f32[15,1024]{1,0:T(8,128)S(1)}, u32[]{:S(2)}, u32[]{:S(2)}) collective-permute-start(f32[15,1024]{1,0:T(8,128)S(1)} %get-tuple-element.51), channel_id=1, source_target_pairs={{0,2},{2,4},{4,6},{6,8},{8,10},{10,12},{12,14},{14,16},{16,18},{18... | collective-permute-start | bytes 184328 | tf_op jit(solution)/shard_map/ppermute | solution.py:15
  50.2 3.8 %concatenate.44 = f32[33,1024]{1,0:T(8,128)S(1)} concatenate(f32[1,1024]{1,0:T(1,128)} %bitcast.160, f32[1,1024]{1,0:T(1,128)} %bitcast.159, f32[1,1024]{1,0:T(1,128)} %bitcast.158, f32[1,1024]{1,0:T(1,128)} %bitcast.157, f32[1,1024]{1,0:T(1,128)} %bitcast.156, f32[1,1024]{1,0:T(1,128)} %bitcast.155, f32[1,1024]{1,0:T(1,128)} %bitcast.154, f32[1,1024]{1,0:T(1,128)} %bitcast.153, ...), dimensions={0} | concatenate | bytes 270336 | tf_op jit(solution)/shard_map/concatenate | solution.py:79
  54.0 0.7 broadcast_multiply_fusion
  54.7 0.0 all-reduce.4.cloned.1.call-update
  54.8 6.9 %fusion.4 = (bf16[256,1024]{1,0:T(8,128)(2,1)}, f32[256,1024]{1,0:T(8,128)}) fusion(bf16[256,1024]{1,0:T(8,128)(2,1)S(1)} %copy-done.3, bf16[256,1024]{1,0:T(8,128)(2,1)S(1)} %copy-done.1, f32[256,1024]{1,0:T(8,128)S(1)} %get-tuple-element.46, f32[15,1024]{1,0:T(8,128)S(1)} %collective-permute-done.3, f32[1024]{0:T(1024)} %bitcast.127, f32[1024]{0:T(1024)} %bitcast.129, ...), kind=kLoop, calls=%fused_computation.35 | loop fusion | flops 26476544 | bytes 3919872 | tf_op jit(solution)/shard_map/convert_element_type | solution.py:89
  61.7 2.3 %multiply_convert_fusion = bf16[256,1024]{1,0:T(8,128)(2,1)} fusion(f32[256,1024]{1,0:T(8,128)} %get-tuple-element.48, bf16[256,1024]{1,0:T(8,128)(2,1)S(1)} %copy-done.1), kind=kLoop, calls=%fused_computation.182 | loop fusion | flops 1572864 | bytes 2097152 | tf_op jit(solution)/shard_map/convert_element_type | solution.py:88
  64.0 101.4 %all-reduce.4.cloned.1.call-done = f32[33,1024]{1,0:T(8,128)} async-done(((f32[33,1024]{1,0:T(8,128)}), f32[33,1024]{1,0:T(8,128)}) %all-reduce.4.cloned.1.call-update) | async-done | bytes 135184 | tf_op jit(solution)/shard_map/psum | solution.py:84
  165.4 1.4 fusion.96
  166.8 1.6 slice.579
  (59 shorter events, 0.2 us)
Async XLA Ops:
  7.2 20.9 %copy-start = (bf16[256,2048]{1,0:T(8,128)(2,1)S(1)}, bf16[256,2048]{1,0:T(8,128)(2,1)}, u32[]{:S(2)}) copy-start(bf16[256,2048]{1,0:T(8,128)(2,1)} %param.13) | copy-start | bytes 3145732
  7.2 158.2 %all-reduce.4.cloned.1.call-start = ((), (), s32[]{:S(2)}) async-start(), calls=%async_computation | async-start | bytes 327680 | tf_op jit(solution)/shard_map/psum | solution.py:84
  8.9 6.5 %collective-permute-start = (bf16[15,1024]{1,0:T(8,128)(2,1)S(1)}, bf16[15,1024]{1,0:T(8,128)(2,1)S(1)}, u32[]{:S(2)}, u32[]{:S(2)}) collective-permute-start(bf16[15,1024]{1,0:T(8,128)(2,1)S(1)} %get-tuple-element.52), channel_id=1, source_target_pairs={{0,2},{2,4},{4,6},{6,8},{8,10},{10,12},{12,14},{14,16},{16,18},{18... | collective-permute-start | bytes 92168 | tf_op jit(solution)/shard_map/ppermute | solution.py:15
  13.7 5.8 %collective-permute-start.1 = (bf16[15,1024]{1,0:T(8,128)(2,1)S(1)}, bf16[15,1024]{1,0:T(8,128)(2,1)S(1)}, u32[]{:S(2)}, u32[]{:S(2)}) collective-permute-start(bf16[15,1024]{1,0:T(8,128)(2,1)S(1)} %get-tuple-element.53), channel_id=1, source_target_pairs={{2,0},{4,2},{6,4},{8,6},{10,8},{12,10},{14,12},{16,14},{18,16},{20... | collective-permute-start | bytes 92168 | tf_op jit(solution)/shard_map/ppermute | solution.py:18
  15.1 10.3 %copy-start.5 = (f32[1,1024]{1,0:T(1,128)}, f32[1,1024]{1,0:T(1,128)S(1)}, u32[]{:S(2)}) copy-start(f32[1,1024]{1,0:T(1,128)S(1)} %get-tuple-element.68) | copy-start | bytes 12292
  15.1 10.3 %copy-start.6 = (f32[1,1024]{1,0:T(1,128)}, f32[1,1024]{1,0:T(1,128)S(1)}, u32[]{:S(2)}) copy-start(f32[1,1024]{1,0:T(1,128)S(1)} %get-tuple-element.69) | copy-start | bytes 12292
  15.1 10.3 %copy-start.7 = (f32[1,1024]{1,0:T(1,128)}, f32[1,1024]{1,0:T(1,128)S(1)}, u32[]{:S(2)}) copy-start(f32[1,1024]{1,0:T(1,128)S(1)} %get-tuple-element.70) | copy-start | bytes 12292
  15.1 10.3 %copy-start.8 = (f32[1,1024]{1,0:T(1,128)}, f32[1,1024]{1,0:T(1,128)S(1)}, u32[]{:S(2)}) copy-start(f32[1,1024]{1,0:T(1,128)S(1)} %get-tuple-element.71) | copy-start | bytes 12292
  15.1 10.3 %copy-start.9 = (f32[1,1024]{1,0:T(1,128)}, f32[1,1024]{1,0:T(1,128)S(1)}, u32[]{:S(2)}) copy-start(f32[1,1024]{1,0:T(1,128)S(1)} %get-tuple-element.72) | copy-start | bytes 12292
  15.2 10.3 %copy-start.10 = (f32[1,1024]{1,0:T(1,128)}, f32[1,1024]{1,0:T(1,128)S(1)}, u32[]{:S(2)}) copy-start(f32[1,1024]{1,0:T(1,128)S(1)} %get-tuple-element.73) | copy-start | bytes 12292
  15.2 10.3 %copy-start.11 = (f32[1,1024]{1,0:T(1,128)}, f32[1,1024]{1,0:T(1,128)S(1)}, u32[]{:S(2)}) copy-start(f32[1,1024]{1,0:T(1,128)S(1)} %get-tuple-element.74) | copy-start | bytes 12292
  15.2 10.3 %copy-start.12 = (f32[1,1024]{1,0:T(1,128)}, f32[1,1024]{1,0:T(1,128)S(1)}, u32[]{:S(2)}) copy-start(f32[1,1024]{1,0:T(1,128)S(1)} %get-tuple-element.75) | copy-start | bytes 12292
  15.2 10.3 %copy-start.13 = (f32[1,1024]{1,0:T(1,128)}, f32[1,1024]{1,0:T(1,128)S(1)}, u32[]{:S(2)}) copy-start(f32[1,1024]{1,0:T(1,128)S(1)} %get-tuple-element.76) | copy-start | bytes 12292
  15.2 10.3 %copy-start.14 = (f32[1,1024]{1,0:T(1,128)}, f32[1,1024]{1,0:T(1,128)S(1)}, u32[]{:S(2)}) copy-start(f32[1,1024]{1,0:T(1,128)S(1)} %get-tuple-element.77) | copy-start | bytes 12292
  15.3 10.3 %copy-start.15 = (f32[1,1024]{1,0:T(1,128)}, f32[1,1024]{1,0:T(1,128)S(1)}, u32[]{:S(2)}) copy-start(f32[1,1024]{1,0:T(1,128)S(1)} %get-tuple-element.78) | copy-start | bytes 12292
  15.3 10.3 %copy-start.16 = (f32[1,1024]{1,0:T(1,128)}, f32[1,1024]{1,0:T(1,128)S(1)}, u32[]{:S(2)}) copy-start(f32[1,1024]{1,0:T(1,128)S(1)} %get-tuple-element.79) | copy-start | bytes 12292
  15.3 10.3 %copy-start.17 = (f32[1,1024]{1,0:T(1,128)}, f32[1,1024]{1,0:T(1,128)S(1)}, u32[]{:S(2)}) copy-start(f32[1,1024]{1,0:T(1,128)S(1)} %get-tuple-element.80) | copy-start | bytes 12292
  15.3 10.3 %copy-start.18 = (f32[1,1024]{1,0:T(1,128)}, f32[1,1024]{1,0:T(1,128)S(1)}, u32[]{:S(2)}) copy-start(f32[1,1024]{1,0:T(1,128)S(1)} %get-tuple-element.81) | copy-start | bytes 12292
  15.3 10.3 %copy-start.19 = (f32[1,1024]{1,0:T(1,128)}, f32[1,1024]{1,0:T(1,128)S(1)}, u32[]{:S(2)}) copy-start(f32[1,1024]{1,0:T(1,128)S(1)} %get-tuple-element.82) | copy-start | bytes 12292
  15.3 10.3 %copy-start.20 = (f32[1,1024]{1,0:T(1,128)}, f32[1,1024]{1,0:T(1,128)S(1)}, u32[]{:S(2)}) copy-start(f32[1,1024]{1,0:T(1,128)S(1)} %get-tuple-element.83) | copy-start | bytes 12292
  43.3 11.4 %copy-start.1 = (bf16[256,1024]{1,0:T(8,128)(2,1)S(1)}, bf16[256,1024]{1,0:T(8,128)(2,1)}, u32[]{:S(2)}) copy-start(bf16[256,1024]{1,0:T(8,128)(2,1)} %param.8) | copy-start | bytes 1572868
  43.3 11.4 %copy-start.3 = (bf16[256,1024]{1,0:T(8,128)(2,1)S(1)}, bf16[256,1024]{1,0:T(8,128)(2,1)}, u32[]{:S(2)}) copy-start(bf16[256,1024]{1,0:T(8,128)(2,1)} %param.7) | copy-start | bytes 1572868
  44.0 10.7 %collective-permute-start.2 = (f32[15,1024]{1,0:T(8,128)}, f32[15,1024]{1,0:T(8,128)S(1)}, u32[]{:S(2)}, u32[]{:S(2)}) collective-permute-start(f32[15,1024]{1,0:T(8,128)} %get-tuple-element.50), channel_id=1, source_target_pairs={{2,0},{4,2},{6,4},{8,6},{10,8},{12,10},{14,12},{16,14},{18,16},{20... | collective-permute-start | bytes 184328 | tf_op jit(solution)/shard_map/ppermute | solution.py:18
  45.3 9.5 %collective-permute-start.3 = (f32[15,1024]{1,0:T(8,128)S(1)}, f32[15,1024]{1,0:T(8,128)S(1)}, u32[]{:S(2)}, u32[]{:S(2)}) collective-permute-start(f32[15,1024]{1,0:T(8,128)S(1)} %get-tuple-element.51), channel_id=1, source_target_pairs={{0,2},{2,4},{4,6},{6,8},{8,10},{10,12},{12,14},{14,16},{16,18},{18... | collective-permute-start | bytes 184328 | tf_op jit(solution)/shard_map/ppermute | solution.py:15
  (7 other events, 63.5 us)
Sparse Core Ops, SparseCore 0:
  54.8 110.4 all-reduce.3
where the time goes:
time: 176 us; the launch traced here: 175 us
  waiting for transfers between devices  106 us (60%)
  other arithmetic  24.5 us (14%)
  between operations  14.5 us (8%)
  starting transfers between devices  12.4 us (7%)
  local copies, waits for them, and re-layouts  7.63 us (4%)
  matrix products  5.53 us (3%)
  blocking collectives  4.91 us (3%)
    psum x1, waiting for transfers between devices, shards(): summed = lax.psum(stacked, 'sp')  101 us
    ppermute x2, starting transfers between devices, with_halo(): lax.ppermute(lax.slice_in_dim(block, block.shape[dim] - width, None, axis...  9.8 us
    reduce_sum x2, other arithmetic, shards(): jnp.sum(own_grad * gated_float[offset:offset + rows], 0)  7.23 us
    convert_element_type x1, other arithmetic, shards(): (grad_gated * value_in.astype(jnp.float32) * gate_sig * (1.0 - gate_sig))...  6.89 us
    reduce_sum x1, other arithmetic, norm_backward(): jnp.sum(conv_out * conv_out, 1)  5.69 us
    dot_general x1, matrix products, norm_backward(): lax.dot_general(grad_rows, w_out, (((1,), (1,)), ((), ())), preferred_ele...  5.53 us
    ppermute x2, waiting for transfers between devices, with_halo(): lax.ppermute(lax.slice_in_dim(block, 0, width, axis=dim), axis, backward)  4.19 us
    concatenate x1, local copies, waits for them, and re-layouts, shards(): jnp.concatenate([tap_terms, jnp.sum(grad_pre * normed, 0)[None], jnp.sum(...  3.82 us
  transfers between devices with their start and end apart: 5, of which 2 were waited for; matrix products, arithmetic and copies ran while one was open for 8% of the time, Pallas kernels for 0%

commit v1 on v0

--- a/solution.py
+++ b/solution.py
@@ -1,10 +1,19 @@
+import functools
 import math
 import jax
 import jax.numpy as jnp
 from jax import lax
 from jax.sharding import PartitionSpec as P
+from jax.lax import all_gather
 
 EPS = 1e-05
+
+
+def words_begin(here_x, axis_key):
+    return jnp.sum(all_gather(here_x, axis_name=axis_key), axis=0)
+
+
+answer_the_slots = functools.partial(words_begin, axis_key="sp")
 
 
 def with_halo(block, sides, width):
@@ -81,7 +90,7 @@
         )
         * scale
     )
-    summed = lax.psum(stacked, "sp")
+    summed = answer_the_slots(stacked)
     d_taps = summed[:kernel]
     d_gain = summed[kernel]
     d_shift = summed[kernel + 1]

time: 176 us -> 122 us (0.69)
  waiting for transfers between devices: 106 us -> 56.2 us
  local copies, waits for them, and re-layouts: 7.63 us -> 3.83 us
    psum x1 -> x0, waiting for transfers between devices: 101 us -> none  [shards(): summed = lax.psum(stacked, 'sp')]
    all_gather x0 -> x1, waiting for transfers between devices: none -> 48.6 us  [words_begin(): return jnp.sum(all_gather(here_x, axis_name=axis_key), axis=0)]
    ppermute x2, waiting for transfers between devices: 0.01 us -> 2.88 us  [with_halo(): lax.ppermute(lax.slice_in_dim(block, block.shape[dim] - width, None, axis...]
    reduce_sum x0 -> x1, other arithmetic: none -> 1.92 us  [words_begin(): return jnp.sum(all_gather(here_x, axis_name=axis_key), axis=0)]
  transfers between devices with their start and end apart: 5 -> 5, of which waited for: 2 -> 5; matrix products, arithmetic and copies ran while one was open for 8% -> 7% of each run, Pallas kernels for 0% -> 0%
where the time goes in v1:
time: 122 us
  waiting for transfers between devices  56.2 us (46%)
  other arithmetic  24.7 us (20%)
  between operations  14.2 us (12%)
  starting transfers between devices  12.4 us (10%)
  matrix products  5.52 us (5%)
  blocking collectives  4.91 us (4%)
  local copies, waits for them, and re-layouts  3.83 us (3%)
    all_gather x1, waiting for transfers between devices, words_begin(): return jnp.sum(all_gather(here_x, axis_name=axis_key), axis=0)  48.6 us
    ppermute x2, starting transfers between devices, with_halo(): lax.ppermute(lax.slice_in_dim(block, block.shape[dim] - width, None, axis...  9.8 us
    reduce_sum x2, other arithmetic, shards(): jnp.sum(own_grad * gated_float[offset:offset + rows], 0)  6.57 us
    convert_element_type x1, other arithmetic, shards(): (grad_gated * value_in.astype(jnp.float32) * gate_sig * (1.0 - gate_sig))...  5.81 us
    reduce_sum x1, other arithmetic, norm_backward(): jnp.sum(conv_out * conv_out, 1)  5.69 us
    dot_general x1, matrix products, norm_backward(): lax.dot_general(grad_rows, w_out, (((1,), (1,)), ((), ())), preferred_ele...  5.52 us
    ppermute x2, waiting for transfers between devices, with_halo(): lax.ppermute(lax.slice_in_dim(block, 0, width, axis=dim), axis, backward)  4.71 us
    ppermute x2, waiting for transfers between devices, with_halo(): lax.ppermute(lax.slice_in_dim(block, block.shape[dim] - width, None, axis...  2.88 us
  transfers between devices with their start and end apart: 5, of which 5 were waited for; matrix products, arithmetic and copies ran while one was open for 7% of the time, Pallas kernels for 0%

profile of v1, /device:TPU:0, one launch (start us, length us, event | category | flops | bytes accessed | tf_op | source)
XLA Modules:
  0.0 121.8 jit_solution(4767323120637284882)
XLA Ops:
  7.2 1.6 %fusion.1 = bf16[256,1024]{1,0:T(8,128)(2,1)S(1)} fusion(bf16[256,1024]{1,0:T(8,128)(2,1)} %param.7, bf16[256,1024]{1,0:T(8,128)(2,1)} %param.8), kind=kLoop, calls=%fused_computation.32 | loop fusion | flops 1835008 | bytes 1572864 | tf_op jit(solution)/shard_map/convert_element_type | solution.py:34
  8.9 4.9 %collective-permute-start = (bf16[15,1024]{1,0:T(8,128)(2,1)S(1)}, bf16[15,1024]{1,0:T(8,128)(2,1)S(1)}, u32[]{:S(2)}, u32[]{:S(2)}) collective-permute-start(bf16[15,1024]{1,0:T(8,128)(2,1)S(1)} %get-tuple-element.52), channel_id=1, source_target_pairs={{0,2},{2,4},{4,6},{6,8},{8,10},{10,12},{12,14},{14,16},{16,18},{18... | collective-permute-start | bytes 92168 | tf_op jit(solution)/shard_map/ppermute | solution.py:24
  13.7 1.3 %collective-permute-start.1 = (bf16[15,1024]{1,0:T(8,128)(2,1)S(1)}, bf16[15,1024]{1,0:T(8,128)(2,1)S(1)}, u32[]{:S(2)}, u32[]{:S(2)}) collective-permute-start(bf16[15,1024]{1,0:T(8,128)(2,1)S(1)} %get-tuple-element.53), channel_id=1, source_target_pairs={{2,0},{4,2},{6,4},{8,6},{10,8},{12,10},{14,12},{16,14},{18,16},{20... | collective-permute-start | bytes 92168 | tf_op jit(solution)/shard_map/ppermute | solution.py:27
  15.2 0.2 collective-permute-done
  15.3 4.2 %collective-permute-done.1 = bf16[15,1024]{1,0:T(8,128)(2,1)S(1)} collective-permute-done((bf16[15,1024]{1,0:T(8,128)(2,1)S(1)}, bf16[15,1024]{1,0:T(8,128)(2,1)S(1)}, u32[]{:S(2)}, u32[]{:S(2)}) %collective-permute-start.1) | collective-permute-done | bytes 30752 | tf_op jit(solution)/shard_map/ppermute | solution.py:27
  19.5 0.2 maximum_convert_fusion
  19.7 5.7 %multiply_reduce_fusion.33 = (f32[256]{0:T(256)S(1)}, f32[256]{0:T(256)S(1)}, f32[256,1024]{1,0:T(8,128)S(1)}) fusion(f32[286,1024]{1,0:T(8,128)S(1)} %maximum_convert_fusion, f32[1024]{0:T(1024)S(1)} %bitcast.126, f32[1024]{0:T(1024)S(1)} %bitcast.128, f32[1024]{0:T(1024)S(1)} %bitcast.70, f32[1024]{0:T(1024)S(1)} %bitcast.72, f32[1024]{0:T(1024)S(1)} %bitcast.74, ...), kind=kLoop, calls=%fused_computation.186 | loop fusion | flops 16776704 | bytes 33683456 | tf_op jit(solution)/shard_map/reduce_sum | solution.py:46
  25.4 2.5 %all-reduce.1 = (f32[256]{0:T(256)S(1)}, f32[256]{0:T(256)S(1)}) all-reduce(f32[256]{0:T(256)S(1)} %get-tuple-element.41, f32[256]{0:T(256)S(1)} %get-tuple-element.40), channel_id=1, replica_groups=mesh['sp'=16,'tp'=2] {'tp'}, use_global_device_ids=true, to_apply=%region_3.0 | all-reduce | flops 512 | bytes 4096 | tf_op jit(solution)/shard_map/psum | solution.py:46
  27.9 5.5 %multiply_reduce_fusion = (f32[1024]{0:T(1024)}, f32[256]{0:T(256)S(1)}, f32[256]{0:T(256)S(1)}, f32[1024]{0:T(1024)}, f32[256,1024]{1,0:T(8,128)}) fusion(f32[256,1024]{1,0:T(8,128)S(1)} %get-tuple-element.49, f32[256]{0:T(256)S(1)} %get-tuple-element.88, f32[256]{0:T(256)S(1)} %get-tuple-element.87, f32[1024]{0:T(1024)S(1)} %copy-done.5, ...), kind=kOutput, calls=%fused_computation.150 | convolution fusion | flops 1078720000 | bytes 7360512 | tf_op jit(solution)/shard_map/dot_general | solution.py:52
  33.5 2.4 %all-reduce = (f32[256]{0:T(256)S(1)}, f32[256]{0:T(256)S(1)}) all-reduce(f32[256]{0:T(256)S(1)} %get-tuple-element.37, f32[256]{0:T(256)S(1)} %get-tuple-element.38), channel_id=1, replica_groups=mesh['sp'=16,'tp'=2] {'tp'}, use_global_device_ids=true, to_apply=%region_7.0 | all-reduce | flops 512 | bytes 4096 | tf_op jit(solution)/shard_map/psum | solution.py:58
  35.9 4.2 %multiply_reduce_fusion.1 = (f32[1024]{0:T(1024)S(1)}, f32[1024]{0:T(1024)S(1)}, f32[1024]{0:T(1024)S(1)}, f32[1024]{0:T(1024)S(1)}, f32[1024]{0:T(1024)S(1)}, /...) fusion(f32[286,1024]{1,0:T(8,128)S(1)} %maximum_convert_fusion,, ...), kind=kLoop, calls=%fused_computation.151 | loop fusion | flops 11515904 | bytes 22102016 | tf_op jit(solution)/shard_map/reduce_sum | solution.py:84
  40.1 2.4 %multiply_reduce_fusion.2 = (f32[1024]{0:T(1024)S(1)}, f32[1024]{0:T(1024)S(1)}, f32[1024]{0:T(1024)S(1)}, f32[1024]{0:T(1024)S(1)}, f32[1024]{0:T(1024)S(1)}, /...) fusion(f32[256,1024]{1,0:T(8,128)S(1)} %get-tuple-element.46, ...), kind=kLoop, calls=%fused_computation.152 | loop fusion | flops 6802432 | bytes 14733312 | tf_op jit(solution)/shard_map/reduce_sum | solution.py:84
  42.5 2.4 %concatenate.150 = f32[1,33,1024]{2,1,0:T(8,128)S(1)} concatenate(f32[1,1,1024]{2,1,0:T(1,128)} %bitcast.160, f32[1,1,1024]{2,1,0:T(1,128)} %bitcast.159, f32[1,1,1024]{2,1,0:T(1,128)S(1)} %bitcast.158, f32[1,1,1024]{2,1,0:T(1,128)S(1)} %bitcast.157, f32[1,1,1024]{2,1,0:T(1,128)S(1)} %bitcast.156, f32[1,1,1024]{2,1,0:T(1,128)S(1)} %bitcast.155, f32[1,1,1024]{2,1,0:T(1,128)S(1)} %bitcast.154, ...), dimensions={1} | concatenate | bytes 270336 | tf_op jit(solution)/shard_map/concatenate | solution.py:88
  44.9 0.7 broadcast_multiply_fusion
  45.6 1.3 %collective-permute-start.2 = (f32[15,1024]{1,0:T(8,128)S(1)}, f32[15,1024]{1,0:T(8,128)S(1)}, u32[]{:S(2)}, u32[]{:S(2)}) collective-permute-start(f32[15,1024]{1,0:T(8,128)S(1)} %get-tuple-element.50), channel_id=1, source_target_pairs={{2,0},{4,2},{6,4},{8,6},{10,8},{12,10},{14,12},{16,14},{18,16},{20... | collective-permute-start | bytes 184328 | tf_op jit(solution)/shard_map/ppermute | solution.py:27
  46.9 4.9 %collective-permute-start.3 = (f32[15,1024]{1,0:T(8,128)S(1)}, f32[15,1024]{1,0:T(8,128)S(1)}, u32[]{:S(2)}, u32[]{:S(2)}) collective-permute-start(f32[15,1024]{1,0:T(8,128)S(1)} %get-tuple-element.51), channel_id=1, source_target_pairs={{0,2},{2,4},{4,6},{6,8},{8,10},{10,12},{12,14},{14,16},{16,18},{18... | collective-permute-start | bytes 184328 | tf_op jit(solution)/shard_map/ppermute | solution.py:24
  51.8 0.5 collective-permute-done.2
  52.3 2.7 %collective-permute-done.3 = f32[15,1024]{1,0:T(8,128)S(1)} collective-permute-done((f32[15,1024]{1,0:T(8,128)S(1)}, f32[15,1024]{1,0:T(8,128)S(1)}, u32[]{:S(2)}, u32[]{:S(2)}) %collective-permute-start.3) | collective-permute-done | bytes 61472 | tf_op jit(solution)/shard_map/ppermute | solution.py:24
  55.0 5.8 %fusion.4 = (bf16[256,1024]{1,0:T(8,128)(2,1)}, f32[256,1024]{1,0:T(8,128)}) fusion(bf16[256,1024]{1,0:T(8,128)(2,1)S(1)} %copy-done.3, bf16[256,1024]{1,0:T(8,128)(2,1)S(1)} %copy-done.1, f32[256,1024]{1,0:T(8,128)S(1)} %get-tuple-element.46, f32[15,1024]{1,0:T(8,128)S(1)} %collective-permute-done.3, f32[1024]{0:T(1024)S(1)} %bitcast.127, ...), kind=kLoop, calls=%fused_computation.35 | loop fusion | flops 26476544 | bytes 3919872 | tf_op jit(solution)/shard_map/convert_element_type | solution.py:98
  60.9 2.3 %multiply_convert_fusion = bf16[256,1024]{1,0:T(8,128)(2,1)} fusion(f32[256,1024]{1,0:T(8,128)} %get-tuple-element.48, bf16[256,1024]{1,0:T(8,128)(2,1)S(1)} %copy-done.1), kind=kLoop, calls=%fused_computation.182 | loop fusion | flops 1572864 | bytes 2097152 | tf_op jit(solution)/shard_map/convert_element_type | solution.py:97
  63.2 48.6 %all-gather.2.cloned.1.call-done = f32[16,33,1024]{2,1,0:T(8,128)} async-done(((f32[1,33,1024]{2,1,0:T(8,128)}), f32[16,33,1024]{2,1,0:T(8,128)}) %all-gather.2.cloned.1.call-update) | async-done | bytes 2162704 | tf_op jit(solution)/shard_map/all_gather | solution.py:13
  111.8 1.9 %reduce_sum.379 = f32[33,1024]{1,0:T(8,128)S(1)} reduce(f32[16,33,1024]{2,1,0:T(8,128)} %all-gather.2.cloned.1.call-done, f32[]{:T(128)} %constant.6.clone.1), dimensions={0}, to_apply=%region_41.0 | reduce | flops 506880 | bytes 2297860 | tf_op jit(solution)/shard_map/reduce_sum | solution.py:13
  113.7 0.6 fusion.96
  114.3 0.7 slice.579
  (22 shorter events, 0.2 us)
Async XLA Ops:
  7.2 20.8 %copy-start = (bf16[256,2048]{1,0:T(8,128)(2,1)S(1)}, bf16[256,2048]{1,0:T(8,128)(2,1)}, u32[]{:S(2)}) copy-start(bf16[256,2048]{1,0:T(8,128)(2,1)} %param.13) | copy-start | bytes 3145732
  7.2 7.9 %copy-start.4 = (f32[31,1024]{1,0:T(8,128)S(1)}, f32[31,1024]{1,0:T(8,128)}, u32[]{:S(2)}) copy-start(f32[31,1024]{1,0:T(8,128)} %param.9) | copy-start | bytes 380932
  7.2 104.6 %all-gather.2.cloned.1.call-start = ((), (), s32[]{:S(2)}) async-start(), calls=%async_computation | async-start | bytes 2785280 | tf_op jit(solution)/shard_map/all_gather | solution.py:13
  8.9 6.5 %collective-permute-start = (bf16[15,1024]{1,0:T(8,128)(2,1)S(1)}, bf16[15,1024]{1,0:T(8,128)(2,1)S(1)}, u32[]{:S(2)}, u32[]{:S(2)}) collective-permute-start(bf16[15,1024]{1,0:T(8,128)(2,1)S(1)} %get-tuple-element.52), channel_id=1, source_target_pairs={{0,2},{2,4},{4,6},{6,8},{8,10},{10,12},{12,14},{14,16},{16,18},{18... | collective-permute-start | bytes 92168 | tf_op jit(solution)/shard_map/ppermute | solution.py:24
  13.7 5.8 %collective-permute-start.1 = (bf16[15,1024]{1,0:T(8,128)(2,1)S(1)}, bf16[15,1024]{1,0:T(8,128)(2,1)S(1)}, u32[]{:S(2)}, u32[]{:S(2)}) collective-permute-start(bf16[15,1024]{1,0:T(8,128)(2,1)S(1)} %get-tuple-element.53), channel_id=1, source_target_pairs={{2,0},{4,2},{6,4},{8,6},{10,8},{12,10},{14,12},{16,14},{18,16},{20... | collective-permute-start | bytes 92168 | tf_op jit(solution)/shard_map/ppermute | solution.py:27
  19.7 8.2 %copy-start.5 = (f32[1024]{0:T(1024)S(1)}, f32[1024]{0:T(1024)}, u32[]{:S(2)}) copy-start(f32[1024]{0:T(1024)} %param.10) | copy-start | bytes 12292
  19.7 8.2 %copy-start.6 = (f32[1024]{0:T(1024)S(1)}, f32[1024]{0:T(1024)}, u32[]{:S(2)}) copy-start(f32[1024]{0:T(1024)} %param.11) | copy-start | bytes 12292
  25.4 8.0 %copy-start.2 = (f32[256,1024]{1,0:T(8,128)}, f32[256,1024]{1,0:T(8,128)S(1)}, u32[]{:S(2)}) copy-start(f32[256,1024]{1,0:T(8,128)S(1)} %get-tuple-element.49) | copy-start | bytes 3145732
  42.5 12.6 %copy-start.1 = (bf16[256,1024]{1,0:T(8,128)(2,1)S(1)}, bf16[256,1024]{1,0:T(8,128)(2,1)}, u32[]{:S(2)}) copy-start(bf16[256,1024]{1,0:T(8,128)(2,1)} %param.8) | copy-start | bytes 1572868
  42.5 12.6 %copy-start.3 = (bf16[256,1024]{1,0:T(8,128)(2,1)S(1)}, bf16[256,1024]{1,0:T(8,128)(2,1)}, u32[]{:S(2)}) copy-start(bf16[256,1024]{1,0:T(8,128)(2,1)} %param.7) | copy-start | bytes 1572868
  45.6 6.7 %collective-permute-start.2 = (f32[15,1024]{1,0:T(8,128)S(1)}, f32[15,1024]{1,0:T(8,128)S(1)}, u32[]{:S(2)}, u32[]{:S(2)}) collective-permute-start(f32[15,1024]{1,0:T(8,128)S(1)} %get-tuple-element.50), channel_id=1, source_target_pairs={{2,0},{4,2},{6,4},{8,6},{10,8},{12,10},{14,12},{16,14},{18,16},{20... | collective-permute-start | bytes 184328 | tf_op jit(solution)/shard_map/ppermute | solution.py:27
  46.9 8.1 %collective-permute-start.3 = (f32[15,1024]{1,0:T(8,128)S(1)}, f32[15,1024]{1,0:T(8,128)S(1)}, u32[]{:S(2)}, u32[]{:S(2)}) collective-permute-start(f32[15,1024]{1,0:T(8,128)S(1)} %get-tuple-element.51), channel_id=1, source_target_pairs={{0,2},{2,4},{4,6},{6,8},{8,10},{10,12},{12,14},{14,16},{16,18},{18... | collective-permute-start | bytes 184328 | tf_op jit(solution)/shard_map/ppermute | solution.py:24
Sparse Core Ops, SparseCore 0:
  45.7 66.0 all-gather.1
